TPU v7x, 32 devices: a whole 2x2x4 slice. The times are simulated.
32 devices in a mesh: sp: 4 (over y, x), tp: 8 (over z, core).
Axes of the slice: x: 2, y: 2, z: 4, core: 2. Of those that a mesh axis runs over, the one named last changes fastest.
Arguments:
- out_gate: bfloat16 [2048, 2048], P('sp', 'tp'), may hold values from -6 to 6
- in_gate: bfloat16 [2048, 2048], P('sp', 'tp'), may hold values from -6 to 6
- conv_input: bfloat16 [2048, 2048], P('sp', 'tp'), may hold values from -6 to 6
- conv_taps: bfloat16 [3, 2048], P(None, 'tp'), may hold values from -3.5 to 3.5
- documents: int32 [2048], P('sp'), may hold values from 0 to 2, never falling along the last dimension, each value on 1 to 1536 neighbouring positions
- out_weight: bfloat16 [2048, 2048], P('tp'), may hold values from -0.125 to 0.125
- residual: bfloat16 [2048, 2048], P(('sp', 'tp')), may hold values from -6 to 6
- norm_gain: bfloat16 [2048], replicated, may hold values from 0.099609375 to 1.8984375
- expert_ids: int32 [2048, 2], P(('sp', 'tp')), may hold values from 0 to 3, all different within a row; in each aligned block of 64 rows (0 to 63, 64 to 127, ...) at most 48 rows name the same one
- route_weights: float32 [2048, 2], P(('sp', 'tp')), may hold values from 0.1 to 1
- gate_weight: bfloat16 [4, 2048, 4096], P('sp', None, 'tp'), may hold values from -0.125 to 0.125
- up_weight: bfloat16 [4, 2048, 4096], P('sp', None, 'tp'), may hold values from -0.125 to 0.125
- down_weight: bfloat16 [4, 4096, 2048], P('sp', 'tp'), may hold values from -0.09375 to 0.09375
Outputs:
- layer_out: bfloat16 [2048, 2048], P(('sp', 'tp'))
Inputs may be any that keep to these rules, and one draw needn't show every extreme that they name: `expert_ids`: A token's two experts differ; in each aligned block of 64 rows no expert is named by more than 48 entries, a bound that some block reaches. `documents`: document numbers never fall along the sequence; a document holds at most 1536 positions.
All inputs are finite; a program needn't handle non-finite values.
Results may differ from a plain program's by a relative error of at most 0.017.
Values may be sent and summed in bfloat16 or wider, within the bound.
A program may use at most 64 MiB of HBM per device.

v0:
```python
import functools

import jax
import jax.numpy as jnp
from jax import lax
from jax.experimental import pallas as pl
from jax.experimental.pallas import tpu as pltpu
from jax.sharding import PartitionSpec as P

EPS = 1e-06


MESH = pl.DeviceIdType.MESH
CHUNK = 16
COLS = 512
UNITS = 256
HALO = 8
STRIP = 64
LANES = 128
VMEM_LIMIT = 63 * 1024 * 1024


def where_am_i(n_sp, nz):
    s, t = lax.axis_index("sp"), lax.axis_index("tp")
    z, c = t // 2, t % 2
    return s, z, c


def greet(s, z, c, n_sp, nz):
    barrier = pltpu.get_barrier_semaphore()
    peers = [(s, 2 * z + 1 - c)]
    peers += [(s, 2 * lax.rem(z + i, nz) + c) for i in range(1, nz)]
    peers += [(lax.rem(s + k, n_sp), 2 * z + c) for k in range(1, n_sp)]
    for peer in peers:
        pl.semaphore_signal(barrier, inc=1, device_id=peer, device_id_type=MESH)
    return lambda: pl.semaphore_wait(barrier, len(peers))


def send(src, dst, send_sem, recv_sem, peer):
    copy = pltpu.make_async_remote_copy(
        src_ref=src,
        dst_ref=dst,
        send_sem=send_sem,
        recv_sem=recv_sem,
        device_id=peer,
        device_id_type=MESH,
    )
    copy.start()
    return copy


def by_rows(rows, body):
    def step(r, carry):
        body(pl.ds(pl.multiple_of(r * CHUNK, CHUNK), CHUNK))
        return carry

    lax.fori_loop(0, rows // CHUNK, step, 0)


def by_columns(width, body):
    def step(r, carry):
        body(pl.ds(pl.multiple_of(r * COLS, COLS), COLS))
        return carry

    lax.fori_loop(0, width // COLS, step, 0)


def slot_hits(meta, s, n_sp, cap):
    rows = meta.shape[1]
    slots = lax.broadcasted_iota(jnp.int32, (n_sp * cap, rows), 0).astype(jnp.float32)
    own = s.astype(jnp.float32)
    hits = []
    for k in range(2):
        ahead = meta[2 * k : 2 * k + 1, :] - own
        ahead = jnp.where(ahead < 0.0, ahead + float(n_sp), ahead)
        hits.append(slots == ahead * float(cap) + meta[2 * k + 1 : 2 * k + 2, :])
    return hits


def describe(routes, meta, n_sp):
    rows = routes.shape[1]
    choice = [routes[0:1, :], routes[1:2, :]]
    expert = lax.broadcasted_iota(jnp.int32, (-(-n_sp // CHUNK) * CHUNK, rows), 0).astype(jnp.float32)
    names = [expert == choice[0], expert == choice[1]]
    named = (names[0] | names[1]).astype(jnp.float32).astype(jnp.bfloat16)
    before = lax.broadcasted_iota(jnp.int32, (rows, rows), 0) < lax.broadcasted_iota(jnp.int32, (rows, rows), 1)
    earlier = jnp.dot(
        named, before.astype(jnp.float32).astype(jnp.bfloat16), preferred_element_type=jnp.float32
    )
    for k in range(2):
        meta[2 * k : 2 * k + 1, :] = choice[k]
        meta[2 * k + 1 : 2 * k + 2, :] = jnp.sum(jnp.where(names[k], earlier, 0.0), axis=0, keepdims=True)
    meta[4:6, :] = routes[2:4, :]
    meta[6:8, :] = jnp.zeros((2, rows), jnp.float32)


def layer_kernel(
    n_sp, nz, cap,
    in_gate, conv_input, out_gate, taps, docs, out_weight, residual, gain, routes, gate_hbm, up_hbm, down_hbm,
    out,
    gate, up, down, signal, long_docs, tail_signal, tail_docs, halo_signal, halo_docs, gated, part, meta, metas,
    hidden, rx, stage, rz, nbuf, routed, gathered, act, half_rx, arrived, mine, combined, zrx,
    w_sem, h_send, h_recv,
    d_send, d_recv, m_send, m_recv, z_send, z_recv, n_send, n_recv, p_send, p_recv, f_send, f_recv,
    e_send, e_recv, r_send, r_recv, b_send, b_recv,
):
    s, z, c = where_am_i(n_sp, nz)
    o = 1 - c
    partner = (s, 2 * z + o)
    rows, width = residual.shape
    length, channels = in_gate.shape
    order = list(range(1, nz)) + [0]
    ahead = [lax.rem(z + i, nz) for i in range(nz)]
    greeted = greet(s, z, c, n_sp, nz)
    loads = [
        pltpu.make_async_copy(src, dst, w_sem.at[i])
        for i, (src, dst) in enumerate([(gate_hbm, gate), (up_hbm, up), (down_hbm, down)])
    ]
    for load in loads:
        load.start()

    tail = slice(length - HALO, length)
    tail_signal[...] = in_gate[tail, :].astype(jnp.float32) * conv_input[tail, :].astype(jnp.float32)
    tail_docs[...] = docs[tail, :]
    greeted()
    following = (lax.rem(s + 1, n_sp), 2 * z + c)
    halo = [
        send(tail_signal, halo_signal, h_send.at[0], h_recv.at[0], following),
        send(tail_docs, halo_docs, h_send.at[1], h_recv.at[1], following),
    ]
    signal[HALO:, :] = in_gate[...].astype(jnp.float32) * conv_input[...].astype(jnp.float32)
    long_docs[HALO:, :] = docs[...]
    describe(routes, meta, n_sp)
    metas[0] = meta[...]
    notes = [send(meta, metas.at[i], m_send.at[i], m_recv.at[i], (s, 2 * ahead[i] + c)) for i in range(1, nz)]
    tap_values = taps[...].astype(jnp.float32)
    for r in list(range(STRIP, length, STRIP)) + [0]:
        if r == 0:
            for copy in halo:
                copy.wait_recv()
            signal[:HALO, :] = halo_signal[...]
            long_docs[:HALO, :] = jnp.where(s == 0, -1.0, halo_docs[...])
        at = [slice(HALO + r - j, HALO + r - j + STRIP) for j in range(3)]
        here = long_docs[at[0], :]
        same = [None] + [long_docs[at[j], :] == here for j in (1, 2)]
        for l in range(0, channels, LANES):
            lane = slice(l, l + LANES)
            conv = tap_values[2:3, lane] * signal[at[0], lane]
            for j in (1, 2):
                conv = conv + jnp.where(same[j], tap_values[2 - j : 3 - j, lane] * signal[at[j], lane], 0.0)
            gated[r : r + STRIP, lane] = (out_gate[r : r + STRIP, lane].astype(jnp.float32) * conv).astype(
                jnp.bfloat16
            )

    def project(cols):
        part[:, cols] = jnp.dot(
            gated[...], out_weight[:, cols], preferred_element_type=jnp.float32
        ).astype(jnp.bfloat16)

    by_columns(width, project)

    def block(at_z, core):
        return pl.multiple_of((2 * at_z + core) * rows, rows)

    halves = {}
    for i in order:
        halves[i] = send(
            part.at[pl.ds(block(ahead[i], o), rows)], rx.at[i], d_send.at[i], d_recv.at[i], partner
        )
    sums = []
    for i in order:
        halves[i].wait_recv()
        if i:

            def add(r, i=i):
                own = part[pl.ds(pl.multiple_of(block(ahead[i], c) + r.start, CHUNK), CHUNK), :]
                stage[i, r, :] = (own.astype(jnp.float32) + rx[i, r, :].astype(jnp.float32)).astype(jnp.bfloat16)

            by_rows(rows, add)
            sums.append(send(stage.at[i], rz.at[i], z_send.at[i], z_recv.at[i], (s, 2 * ahead[i] + c)))
    for copy in sums:
        copy.wait_recv()

    def norm(r):
        own = part[pl.ds(pl.multiple_of(block(z, c) + r.start, CHUNK), CHUNK), :]
        total = own.astype(jnp.float32) + rx[0, r, :].astype(jnp.float32)
        for i in range(1, nz):
            total = total + rz[i, r, :].astype(jnp.float32)
        state = (residual[r, :].astype(jnp.float32) + total).astype(jnp.bfloat16)
        hidden[r, :] = state
        wide = state.astype(jnp.float32)
        stats = jnp.mean(wide * wide, axis=-1, keepdims=True)
        nbuf[0, r, :] = (wide * lax.rsqrt(stats + EPS) * gain[...].astype(jnp.float32)).astype(jnp.bfloat16)

    by_rows(rows, norm)
    spread = [
        send(nbuf.at[0], nbuf.at[i], n_send.at[i], n_recv.at[i], (s, 2 * ahead[i] + c)) for i in range(1, nz)
    ]

    sent, forwards, swaps, returns, back = {}, {}, {}, {}, []

    def build(i):
        if i:
            notes[i - 1].wait_recv()
            spread[i - 1].wait_recv()
        first, second = slot_hits(metas[i], s, n_sp, cap)
        table = (first | second).astype(jnp.float32).astype(jnp.bfloat16)

        def place(cols):
            placed = jnp.dot(table, nbuf[i, :, cols], preferred_element_type=jnp.float32).astype(jnp.bfloat16)
            gathered[i, 0, 0, :, cols] = placed[:cap]
            for k in range(1, n_sp):
                routed[i, k, :, cols] = placed[k * cap : (k + 1) * cap]

        by_columns(width, place)
        sent[i] = [
            send(
                routed.at[i, k], gathered.at[i, 0, k], p_send.at[i, k], p_recv.at[i, k],
                (lax.rem(s + k, n_sp), 2 * z + c),
            )
            for k in range(1, n_sp)
        ]

    def forward(i):
        for copy in sent[i]:
            copy.wait_recv()
        forwards[i] = send(gathered.at[i, 0], gathered.at[i, 1], f_send.at[i], f_recv.at[i], partner)

    def expert(i):
        if i == 0:
            for load in loads:
                load.wait()
        forwards[i].wait_recv()
        half = n_sp * cap
        hidden_units = gate.shape[1]
        step = min(UNITS, hidden_units)

        def inner(r, carry):
            units = pl.ds(pl.multiple_of(r * step, step), step)
            held = gathered[i].reshape(2 * half, width)
            gate_proj = jnp.dot(held, gate[:, units], preferred_element_type=jnp.float32)
            up_proj = jnp.dot(held, up[:, units], preferred_element_type=jnp.float32)
            act[:, units] = (gate_proj / (1.0 + jnp.exp(-gate_proj)) * up_proj).astype(jnp.bfloat16)
            return carry

        lax.fori_loop(0, hidden_units // step, inner, 0)
        for copy in sent[i]:
            copy.wait_send()
        forwards[i].wait_send()

        def outer(cols):
            share = jnp.dot(act[...], down[:, cols], preferred_element_type=jnp.float32).astype(jnp.bfloat16)
            routed[i, :, :, cols] = share[:half].reshape(n_sp, cap, COLS)
            gathered[i, 0, :, :, cols] = share[half:].reshape(n_sp, cap, COLS)

        by_columns(width, outer)
        swaps[i] = send(gathered.at[i, 0], half_rx.at[i], e_send.at[i], e_recv.at[i], partner)

    def give_back(i):
        swaps[i].wait_recv()

        def add(cols):
            total = routed[i, :, :, cols].astype(jnp.float32) + half_rx[i, :, :, cols].astype(jnp.float32)
            routed[i, :, :, cols] = total.astype(jnp.bfloat16)

        by_columns(width, add)
        returns[i] = [
            send(
                routed.at[i, k], arrived.at[i, k], r_send.at[i, k], r_recv.at[i, k],
                (lax.rem(s + n_sp - k, n_sp), 2 * z + c),
            )
            for k in range(1, n_sp)
        ]

    def combine(i):
        for copy in returns[i]:
            copy.wait_recv()
        weight_rows = metas[i]
        first, second = slot_hits(weight_rows, s, n_sp, cap)
        weights = jnp.where(first, weight_rows[4:5, :], 0.0) + jnp.where(second, weight_rows[5:6, :], 0.0)
        high = weights.astype(jnp.bfloat16)
        low = (weights - high.astype(jnp.float32)).astype(jnp.bfloat16)

        def weigh(cols):
            values = jnp.concatenate(
                [routed[i, 0, :, cols]] + [arrived[i, k, :, cols] for k in range(1, n_sp)], axis=0
            )
            dims = (((0,), (0,)), ((), ()))
            total = lax.dot_general(high, values, dims, preferred_element_type=jnp.float32)
            total = total + lax.dot_general(low, values, dims, preferred_element_type=jnp.float32)
            if i:
                combined[i, :, cols] = total.astype(jnp.bfloat16)
            else:
                mine[:, cols] = total

        by_columns(width, weigh)
        if i:
            back.append(
                send(
                    combined.at[i], zrx.at[i], b_send.at[i], b_recv.at[i], (s, 2 * lax.rem(z + nz - i, nz) + c)
                )
            )

    for i in range(nz):
        build(i)
        if i >= 1:
            forward(i - 1)
        if i >= 2:
            expert(i - 2)
            if i >= 3:
                give_back(i - 2)
    forward(nz - 1)
    for i in range(max(nz - 2, 0), nz):
        expert(i)
        if i:
            give_back(i)
    give_back(0)
    for i in order:
        combine(i)
    for copy in back:
        copy.wait_recv()

    def finish(r):
        total = mine[r, :]
        for i in range(1, nz):
            total = total + zrx[i, r, :].astype(jnp.float32)
        out[r, :] = (hidden[r, :].astype(jnp.float32) + total).astype(jnp.bfloat16)

    by_rows(rows, finish)
    left = halo + list(halves.values()) + notes + sums + spread + list(swaps.values()) + back
    for copy in left + sum(returns.values(), []):
        copy.wait_send()


def shards(
    out_gate,
    in_gate,
    conv_input,
    conv_taps,
    documents,
    out_weight,
    residual,
    norm_gain,
    expert_ids,
    route_weights,
    gate_weight,
    up_weight,
    down_weight,
):
    n_sp, nz = lax.axis_size("sp"), lax.axis_size("tp") // 2
    length, channels = conv_input.shape
    rows, width = residual.shape
    units = gate_weight.shape[2]
    capacity = max(2, (3 * rows + n_sp - 1) // n_sp)
    cap = -(-capacity // CHUNK) * CHUNK
    docs = jnp.broadcast_to(documents.astype(jnp.float32)[:, None], (length, LANES))
    routes = jnp.concatenate([expert_ids.astype(jnp.float32).T, route_weights.T], axis=0)
    bf16, f32, dma = jnp.bfloat16, jnp.float32, pltpu.SemaphoreType.DMA
    vmem, hbm = pl.BlockSpec(memory_space=pltpu.VMEM), pl.BlockSpec(memory_space=pltpu.HBM)
    per_z = pltpu.VMEM((nz, rows, width), bf16)
    slots = pltpu.VMEM((nz, n_sp, cap, width), bf16)
    return pl.pallas_call(
        functools.partial(layer_kernel, n_sp, nz, cap),
        out_shape=jax.ShapeDtypeStruct((rows, width), bf16),
        in_specs=[vmem] * 9 + [hbm] * 3,
        out_specs=vmem,
        scratch_shapes=[
            pltpu.VMEM((width, units), bf16),
            pltpu.VMEM((width, units), bf16),
            pltpu.VMEM((units, width), bf16),
            pltpu.VMEM((HALO + length, channels), f32),
            pltpu.VMEM((HALO + length, LANES), f32),
            pltpu.VMEM((HALO, channels), f32),
            pltpu.VMEM((HALO, LANES), f32),
            pltpu.VMEM((HALO, channels), f32),
            pltpu.VMEM((HALO, LANES), f32),
            pltpu.VMEM((length, channels), bf16),
            pltpu.VMEM((length, width), bf16),
            pltpu.VMEM((8, rows), f32),
            pltpu.VMEM((nz, 8, rows), f32),
            pltpu.VMEM((rows, width), bf16),
            per_z,
            per_z,
            per_z,
            per_z,
            slots,
            pltpu.VMEM((nz, 2, n_sp, cap, width), bf16),
            pltpu.VMEM((2 * n_sp * cap, units), bf16),
            slots,
            slots,
            pltpu.VMEM((rows, width), f32),
            per_z,
            per_z,
            dma((3,)),
            dma((2,)),
            dma((2,)),
        ]
        + [dma((nz,))] * 8
        + [dma((nz, n_sp))] * 2
        + [dma((nz,))] * 4
        + [dma((nz, n_sp))] * 2
        + [dma((nz,))] * 2,
        compiler_params=pltpu.CompilerParams(
            collective_id=0, has_side_effects=True, vmem_limit_bytes=VMEM_LIMIT
        ),
    )(
        in_gate, conv_input, out_gate, conv_taps, docs, out_weight, residual, norm_gain[None, :], routes,
        gate_weight[0], up_weight[0], down_weight[0],
    )


def solution(mesh):
    in_specs = (
        P("sp", "tp"),
        P("sp", "tp"),
        P("sp", "tp"),
        P(None, "tp"),
        P("sp"),
        P("tp", None),
        P(("sp", "tp"), None),
        P(),
        P(("sp", "tp"), None),
        P(("sp", "tp"), None),
        P("sp", None, "tp"),
        P("sp", None, "tp"),
        P("sp", "tp", None),
    )
    out_specs = P(("sp", "tp"), None)
    return jax.shard_map(shards, mesh=mesh, in_specs=in_specs, out_specs=out_specs, check_vma=False)
```

profile of v0, /device:TPU:0, one launch (start us, length us, event | category | flops | bytes accessed | tf_op | source)
XLA Modules:
  0.0 128.5 jit_solution(1636112828681913611)
XLA Ops:
  0.0 0.7 convert_bitcast_fusion
  0.7 1.3 pad_maximum_fusion.routes
  1.9 0.7 convert_element_type.6
  2.6 1.3 broadcast_in_dim.10.gain
  3.9 0.8 broadcast_in_dim.4.docs
  4.7 122.0 %shard_map.127 = bf16[64,2048]{1,0:T(8,128)(2,1)} custom-call(bf16[512,256]{1,0:T(8,128)(2,1)} %in_gate.1, bf16[512,256]{1,0:T(8,128)(2,1)} %conv_input.1, bf16[512,256]{1,0:T(8,128)(2,1)} %out_gate.1, bf16[3,256]{1,0:T(4,128)(2,1)} %taps.1, f32[512,128]{1,0:T(8,128)} %broadcast_in_dim.4.docs, bf16[256,2048]{1,0:T(8,128)(2,1)} %out_weight.1, ...), custom_call_target="tpu_custom_call" | custom-call | tf_op jit(solution)/shard_map/pallas_call | solution.py:362
  126.8 1.7 %copy.15 = bf16[64,2048]{1,0:T(8,128)(2,1)} copy(bf16[64,2048]{1,0:T(8,128)(2,1)} %shard_map.127) | data formatting | bytes 524288
where the time goes:
time: 129 us; the launch traced here: 128 us
  Pallas kernels  122 us (95%)
  local copies, waits for them, and re-layouts  3.79 us (3%)
  other arithmetic  2.63 us (2%)
    pallas_call x1, Pallas kernels, shards(): pl.pallas_call(functools.partial(layer_kernel, n_sp, nz, cap), out_shape=...  122 us

commit v1 on v0

v1 whole, which is shorter than its diff:
```python
import functools

import jax
import jax.numpy as jnp
from jax import lax
from jax.experimental import pallas as pl
from jax.experimental.pallas import tpu as pltpu
from jax.sharding import PartitionSpec as P

EPS = 1e-06


MESH = pl.DeviceIdType.MESH
CHUNK = 16
COLS = 512
UNITS = 256
HALO = 8
PIECE = 32
LAG = 2
LANES = 128
VMEM_LIMIT = 63 * 1024 * 1024


def where_am_i():
    s, t = lax.axis_index("sp"), lax.axis_index("tp")
    return s, t // 2, t % 2


def greet(s, z, c, n_sp, nz):
    barrier = pltpu.get_barrier_semaphore()
    peers = [(s, 2 * z + 1 - c)]
    peers += [(s, 2 * lax.rem(z + i, nz) + c) for i in range(1, nz)]
    peers += [(lax.rem(s + k, n_sp), 2 * z + c) for k in range(1, n_sp)]
    for peer in peers:
        pl.semaphore_signal(barrier, inc=1, device_id=peer, device_id_type=MESH)
    return lambda: pl.semaphore_wait(barrier, len(peers))


def link(src, dst, send_sem, recv_sem, peer):
    return pltpu.make_async_remote_copy(
        src_ref=src,
        dst_ref=dst,
        send_sem=send_sem,
        recv_sem=recv_sem,
        device_id=peer,
        device_id_type=MESH,
    )


def by_rows(first, count, body):
    def step(r, carry):
        body(pl.ds(pl.multiple_of(first + r * CHUNK, CHUNK), CHUNK))
        return carry

    lax.fori_loop(0, count // CHUNK, step, 0)


def by_columns(width, body):
    def step(r, carry):
        body(pl.ds(pl.multiple_of(r * COLS, COLS), COLS))
        return carry

    lax.fori_loop(0, width // COLS, step, 0)


def slot_hits(meta, experts, cap):
    rows = meta.shape[1]
    slots = lax.broadcasted_iota(jnp.int32, (len(experts) * cap, rows), 0).astype(jnp.float32)
    hits = []
    for k in range(2):
        at = jnp.full((1, rows), -1.0, jnp.float32)
        for a, expert in enumerate(experts):
            at = jnp.where(meta[2 * k : 2 * k + 1, :] == expert, float(a * cap) + meta[2 * k + 1 : 2 * k + 2, :], at)
        hits.append(slots == at)
    return hits


def slot_table(meta, experts, cap):
    first, second = slot_hits(meta, experts, cap)
    return (first | second).astype(jnp.float32).astype(jnp.bfloat16)


def slot_weights(meta, experts, cap):
    first, second = slot_hits(meta, experts, cap)
    weights = jnp.where(first, meta[4:5, :], 0.0) + jnp.where(second, meta[5:6, :], 0.0)
    high = weights.astype(jnp.bfloat16)
    return high, (weights - high.astype(jnp.float32)).astype(jnp.bfloat16)


def weigh(weights, values):
    dims = (((0,), (0,)), ((), ()))
    total = lax.dot_general(weights[0], values, dims, preferred_element_type=jnp.float32)
    return total + lax.dot_general(weights[1], values, dims, preferred_element_type=jnp.float32)


def describe(ids, shares, meta, n_sp):
    rows = ids.shape[1]
    named_ids = ids[...].astype(jnp.float32)
    choice = [named_ids[0:1, :], named_ids[1:2, :]]
    expert = lax.broadcasted_iota(jnp.int32, (-(-n_sp // CHUNK) * CHUNK, rows), 0).astype(jnp.float32)
    names = [expert == choice[0], expert == choice[1]]
    named = (names[0] | names[1]).astype(jnp.float32).astype(jnp.bfloat16)
    before = lax.broadcasted_iota(jnp.int32, (rows, rows), 0) < lax.broadcasted_iota(jnp.int32, (rows, rows), 1)
    earlier = jnp.dot(
        named, before.astype(jnp.float32).astype(jnp.bfloat16), preferred_element_type=jnp.float32
    )
    for k in range(2):
        meta[2 * k : 2 * k + 1, :] = choice[k]
        meta[2 * k + 1 : 2 * k + 2, :] = jnp.sum(jnp.where(names[k], earlier, 0.0), axis=0, keepdims=True)
    meta[4:6, :] = shares[...]
    meta[6:8, :] = jnp.zeros((2, rows), jnp.float32)


def layer_kernel(
    n_sp, nz, cap,
    in_gate_hbm, conv_input_hbm, out_gate_hbm, taps_hbm, docs_hbm, out_weight_hbm, residual_hbm, gain_hbm, ids_hbm,
    shares_hbm, gate_hbm, up_hbm, down_hbm,
    out,
    in_gate, conv_input, out_gate, taps, docs, residual, gain, ids, shares, gate, up, down,
    signal, long_docs, tail_signal, tail_docs, halo_signal, halo_docs,
    gated, other_gated, weight, part, from_low, from_high, to_high, to_low, hidden, nbuf,
    meta, metas, side_metas, raw, routed, gathered, act, half_rx, arrived, side_sum, side_rx, mine, combined, zrx,
    w_sem, h_send, h_recv, m_send, m_recv, x_send, x_recv, v_send, v_recv, o_send, o_recv,
    u_send, u_recv, d_send, d_recv, g_send, g_recv, p_send, p_recv, f_send, f_recv,
    e_send, e_recv, r_send, r_recv, k_send, k_recv, b_send, b_recv,
):
    s, z, c = where_am_i()
    o = 1 - c
    relayed = n_sp == 4
    partner = (s, 2 * z + o)
    rows, width = residual.shape
    length, channels = in_gate.shape
    piece = min(PIECE, rows)
    per = rows // piece
    pieces = nz * per
    greeted = greet(s, z, c, n_sp, nz)
    loads = [
        pltpu.make_async_copy(src, dst, w_sem.at[i])
        for i, (src, dst) in enumerate(
            [
                (in_gate_hbm, in_gate), (conv_input_hbm, conv_input), (docs_hbm, docs), (taps_hbm, taps),
                (ids_hbm, ids), (shares_hbm, shares), (out_gate_hbm, out_gate), (out_weight_hbm, weight.at[0]),
                (residual_hbm, residual), (gain_hbm, gain), (gate_hbm, gate), (up_hbm, up), (down_hbm, down),
            ]
        )
    ]
    for load in loads:
        load.start()

    @pl.when(z == 0)
    def no_lower():
        from_low[...] = jnp.zeros_like(from_low)

    @pl.when(z == nz - 1)
    def no_higher():
        from_high[...] = jnp.zeros_like(from_high)

    def above(i):
        return lax.rem(z + i, nz)

    def on_plane(k):
        return lax.rem(s + k, n_sp)

    if relayed:
        right, down_one = 1 - 2 * (s % 2), 2 - 4 * (s // 2)
        side = s + (1 - c) * right + c * down_one
        cross = s + c * right + (1 - c) * down_one
        side_peer, cross_peer = (side, 2 * z + c), (cross, 2 * z + c)
        experts = [s.astype(jnp.float32), cross.astype(jnp.float32)]
    else:
        experts = [on_plane(k).astype(jnp.float32) for k in range(n_sp)]

    for load in loads[:6]:
        load.wait()
    signal[HALO:, :] = in_gate[...].astype(jnp.float32) * conv_input[...].astype(jnp.float32)
    row = jnp.broadcast_to(docs[...].astype(jnp.float32).reshape(1, length), (CHUNK, length))
    one = (lax.broadcasted_iota(jnp.int32, (CHUNK, LANES), 0) == 0).astype(jnp.float32).astype(jnp.bfloat16)
    long_docs[HALO:, :] = lax.dot_general(
        row.astype(jnp.bfloat16), one, (((0,), (0,)), ((), ())), preferred_element_type=jnp.float32
    )
    tail_signal[...] = signal[length : length + HALO, :]
    tail_docs[...] = long_docs[length : length + HALO, :]
    describe(ids, shares, meta, n_sp)
    metas[z] = meta[...]
    loads[6].wait()
    tap_values = taps[...].astype(jnp.float32)

    def convolve(strip):
        r = strip * rows
        at = [slice(HALO + r - j, HALO + r - j + rows) for j in range(3)]
        here = long_docs[at[0], :]
        same = [None] + [long_docs[at[j], :] == here for j in (1, 2)]
        for l in range(0, channels, LANES):
            lane = slice(l, l + LANES)
            conv = tap_values[2:3, lane] * signal[at[0], lane]
            for j in (1, 2):
                conv = conv + jnp.where(same[j], tap_values[2 - j : 3 - j, lane] * signal[at[j], lane], 0.0)
            gated[strip, :, lane] = (out_gate[r : r + rows, lane].astype(jnp.float32) * conv).astype(jnp.bfloat16)

    for strip in range(2 * nz - 1, 0, -1):
        convolve(strip)
    loads[7].wait()
    greeted()
    following = (on_plane(1), 2 * z + c)
    halo = [
        link(tail_signal, halo_signal, h_send.at[0], h_recv.at[0], following),
        link(tail_docs, halo_docs, h_send.at[1], h_recv.at[1], following),
    ]
    given = [
        link(gated.at[2 * b + o], other_gated.at[b], o_send.at[b], o_recv.at[b], partner) for b in range(nz)
    ]
    lent = link(weight.at[0], weight.at[1], v_send.at[0], v_recv.at[0], partner)
    given[nz - 1].start()
    lent.start()
    for copy in halo:
        copy.start()
    for b in range(nz - 2, 0, -1):
        given[b].start()

    def note(i):
        return link(meta, metas.at[z], m_send.at[i], m_recv.at[z], (s, 2 * above(i) + c))

    def noted(i):
        return link(meta, metas.at[above(i)], m_send.at[i], m_recv.at[above(i)], (s, 2 * above(i) + c))

    for i in range(1, nz):
        note(i).start()
    side_note = link(metas, side_metas, x_send.at[0], x_recv.at[0], side_peer) if relayed else None

    def place(q):
        return nz - 1 - q // per, (q % per) * piece

    def upward(q):
        b, first = place(q)
        at = pl.ds(first, piece)
        return link(to_high.at[b, at], from_low.at[b, at], u_send.at[q], u_recv.at[q], (s, 2 * above(1) + c))

    def downward(q):
        b, first = place(q)
        at = pl.ds(first, piece)
        return link(to_low.at[b, at], from_high.at[b, at], d_send.at[q], d_recv.at[q], (s, 2 * above(nz - 1) + c))

    def pass_on(q, came, going, copy):
        b, first = place(q)

        def add(r):
            going[b, r, :] = (part[b, r, :] + came[b, r, :].astype(jnp.float32)).astype(jnp.bfloat16)

        by_rows(first, piece, add)
        copy(q).start()

    def project(b):
        given[b].wait_recv()

        def columns(cols):
            part[b, :, cols] = jnp.dot(
                gated[2 * b + c], weight[0, :, cols], preferred_element_type=jnp.float32
            ) + jnp.dot(other_gated[b], weight[1, :, cols], preferred_element_type=jnp.float32)

        by_columns(width, columns)

        @pl.when(z == b)
        def own():
            def add(r):
                part[b, r, :] = part[b, r, :] + residual[r, :].astype(jnp.float32)

            by_rows(0, rows, add)

    lent.wait_recv()
    loads[8].wait()
    for b in range(nz - 1, -1, -1):
        if b == 0:
            for copy in halo:
                copy.wait_recv()
            signal[:HALO, :] = halo_signal[...]
            long_docs[:HALO, :] = jnp.where(s == 0, -1.0, halo_docs[...])
            convolve(0)
            given[0].start()
        project(b)
        for q in range((nz - 1 - b) * per, (nz - b) * per):

            @pl.when(z == 0)
            def lowest(q=q):
                pass_on(q, from_low, to_high, upward)

            @pl.when(z == nz - 1)
            def highest(q=q):
                pass_on(q, from_high, to_low, downward)

    for i in range(1, nz):
        noted(i).wait_recv()
    if relayed:
        side_note.start()
    loads[9].wait()

    def from_below(q):
        @pl.when(z > 0)
        def some():
            upward(q).wait_recv()

        @pl.when((z > 0) & (z < nz - 1))
        def middle():
            pass_on(q, from_low, to_high, upward)

    def from_above(q):
        @pl.when(z < nz - 1)
        def some():
            downward(q).wait_recv()

        @pl.when((z > 0) & (z < nz - 1))
        def middle():
            pass_on(q, from_high, to_low, downward)

    def norm(q):
        b, first = place(q)

        def rows_of(r):
            total = part[b, r, :] + from_low[b, r, :].astype(jnp.float32) + from_high[b, r, :].astype(jnp.float32)
            state = total.astype(jnp.bfloat16)
            hidden[b, r, :] = state
            wide = state.astype(jnp.float32)
            stats = jnp.mean(wide * wide, axis=-1, keepdims=True)
            scale = gain[...].astype(jnp.float32).reshape(1, width)
            nbuf[b, r, :] = (wide * lax.rsqrt(stats + EPS) * scale).astype(jnp.bfloat16)

        by_rows(first, piece, rows_of)

    def raw_copy(b):
        return link(nbuf.at[b], raw.at[b], g_send.at[b], g_recv.at[b], side_peer)

    def slot_copies(b, those=(0, 1)):
        if relayed:
            return [
                link(routed.at[b, k], gathered.at[b, 0, 2 + k], p_send.at[b, k], p_recv.at[b, k], cross_peer)
                for k in those
            ]
        return [
            link(
                routed.at[b, k], gathered.at[b, 0, k], p_send.at[b, k], p_recv.at[b, k], (on_plane(k), 2 * z + c)
            )
            for k in range(1, n_sp)
        ]

    def dispatch(b):
        if relayed:
            raw_copy(b).start()
        table = slot_table(metas[b], experts, cap)

        def columns(cols):
            placed = jnp.dot(table, nbuf[b, :, cols], preferred_element_type=jnp.float32).astype(jnp.bfloat16)
            gathered[b, 0, 0, :, cols] = placed[:cap]
            for k in range(1, len(experts)):
                routed[b, k - 1 if relayed else k, :, cols] = placed[k * cap : (k + 1) * cap]

        by_columns(width, columns)
        for copy in slot_copies(b, (0,)):
            copy.start()

    def relay(b):
        if not relayed:
            return
        raw_copy(b).wait_recv()
        table = slot_table(side_metas[b], experts, cap)

        def columns(cols):
            placed = jnp.dot(table, raw[b, :, cols], preferred_element_type=jnp.float32).astype(jnp.bfloat16)
            gathered[b, 0, 1, :, cols] = placed[:cap]
            routed[b, 1, :, cols] = placed[cap:]

        by_columns(width, columns)
        slot_copies(b, (1,))[0].start()

    def unless_own(b, act_on):
        @pl.when(z != b)
        def other():
            act_on(b)

    for t in range(pieces + LAG):

        @pl.when(z < nz // 2)
        def lower(t=t):
            if t < pieces:
                from_below(t)
            if t >= LAG:
                from_above(t - LAG)

        @pl.when(z >= nz // 2)
        def upper(t=t):
            if t < pieces:
                from_above(t)
            if t >= LAG:
                from_below(t - LAG)

        q = t - LAG
        if q >= 0:
            if q == 0 and relayed:
                side_note.wait_recv()
            norm(q)
            if q % per == per - 1:
                b = place(q)[0]
                unless_own(b, dispatch)
                if b < nz - 1:
                    unless_own(b + 1, relay)
    dispatch(z)
    unless_own(0, relay)
    relay(z)

    def at_step(j):
        if j == nz - 1:
            return z
        return nz - 1 - j - jnp.where(j >= nz - 1 - z, 1, 0)

    def forward(b):
        return link(gathered.at[b, 0], gathered.at[b, 1], f_send.at[b], f_recv.at[b], partner)

    def swap(b):
        return link(gathered.at[b, 0], half_rx.at[b], e_send.at[b], e_recv.at[b], partner)

    def return_copies(b):
        if relayed:
            return [
                link(routed.at[b, pl.ds(2, 2)], arrived.at[b], r_send.at[b, 0], r_recv.at[b, 0], cross_peer)
            ]
        return [
            link(
                routed.at[b, k], arrived.at[b, k], r_send.at[b, k], r_recv.at[b, k], (on_plane(n_sp - k), 2 * z + c)
            )
            for k in range(1, n_sp)
        ]

    def side_copy(b):
        return link(side_sum.at[b], side_rx.at[b], k_send.at[b], k_recv.at[b], side_peer)

    def gather(j):
        b = at_step(j)
        for copy in slot_copies(b):
            copy.wait_recv()
        forward(b).start()

    def expert(j):
        b = at_step(j)
        if j == 0:
            for load in loads[10:]:
                load.wait()
        forward(b).wait_recv()
        half = n_sp * cap
        hidden_units = gate.shape[1]
        step = min(UNITS, hidden_units)

        def inner(r, carry):
            units = pl.ds(pl.multiple_of(r * step, step), step)
            held = gathered[b].reshape(2 * half, width)
            gate_proj = jnp.dot(held, gate[:, units], preferred_element_type=jnp.float32)
            up_proj = jnp.dot(held, up[:, units], preferred_element_type=jnp.float32)
            act[:, units] = (gate_proj / (1.0 + jnp.exp(-gate_proj)) * up_proj).astype(jnp.bfloat16)
            return carry

        lax.fori_loop(0, hidden_units // step, inner, 0)
        for copy in slot_copies(b):
            copy.wait_send()
        forward(b).wait_send()

        def outer(cols):
            share = jnp.dot(act[...], down[:, cols], preferred_element_type=jnp.float32).astype(jnp.bfloat16)
            routed[b, :, :, cols] = share[:half].reshape(n_sp, cap, COLS)
            gathered[b, 0, :, :, cols] = share[half:].reshape(n_sp, cap, COLS)

        by_columns(width, outer)
        swap(b).start()

    def give_back(j):
        b = at_step(j)
        swap(b).wait_recv()

        def add(first, count):
            def columns(cols):
                at = pl.ds(first, count)
                total = routed[b, at, :, cols].astype(jnp.float32) + half_rx[b, at, :, cols].astype(jnp.float32)
                routed[b, at, :, cols] = total.astype(jnp.bfloat16)

            by_columns(width, columns)

        if relayed:
            add(2, 2)
        else:
            add(0, n_sp)
        for copy in return_copies(b):
            copy.start()
        if relayed:
            add(0, 2)

    def relay_back(j):
        if not relayed:
            return
        b = at_step(j)
        return_copies(b)[0].wait_recv()
        weights = slot_weights(side_metas[b], experts, cap)

        def columns(cols):
            values = jnp.concatenate([routed[b, 1, :, cols], arrived[b, 1, :, cols]], axis=0)
            side_sum[b, :, cols] = weigh(weights, values).astype(jnp.bfloat16)

        by_columns(width, columns)
        side_copy(b).start()

    def homeward(b):
        return link(combined.at[b], zrx.at[z], b_send.at[b], b_recv.at[z], (s, 2 * b + c))

    def collect(j):
        b = at_step(j)
        if relayed:
            side_copy(b).wait_recv()
        else:
            for copy in return_copies(b):
                copy.wait_recv()
        weights = slot_weights(metas[b], experts, cap)

        def columns(cols):
            parts = [routed[b, 0, :, cols]]
            if relayed:
                parts.append(arrived[b, 0, :, cols])
            else:
                parts += [arrived[b, k, :, cols] for k in range(1, n_sp)]
            total = weigh(weights, jnp.concatenate(parts, axis=0))
            if relayed:
                total = total + side_rx[b, :, cols].astype(jnp.float32)
            if j < nz - 1:
                combined[b, :, cols] = total.astype(jnp.bfloat16)
            else:
                mine[:, cols] = total

        by_columns(width, columns)
        if j < nz - 1:
            homeward(b).start()

    gather(0)
    for j in range(nz):
        if j + 1 < nz:
            gather(j + 1)
        expert(j)
        if j >= 1:
            relay_back(j - 1)
        give_back(j)
        if j >= 2:
            collect(j - 2)
    relay_back(nz - 1)
    if nz > 1:
        collect(nz - 2)
    collect(nz - 1)

    def home(i):
        return link(combined.at[z], zrx.at[above(i)], b_send.at[above(i)], b_recv.at[above(i)], (s, 2 * above(i) + c))

    for i in range(1, nz):
        home(i).wait_recv()

    def finish(r):
        total = mine[r, :]
        for i in range(1, nz):
            total = total + zrx[above(i), r, :].astype(jnp.float32)
        out[r, :] = (hidden[z, r, :].astype(jnp.float32) + total).astype(jnp.bfloat16)

    by_rows(0, rows, finish)
    left = halo + given + [lent] + [note(i) for i in range(1, nz)]
    if relayed:
        left += [side_note] + [raw_copy(b) for b in range(nz)] + [side_copy(b) for b in range(nz)]
    left += [swap(b) for b in range(nz)] + sum([return_copies(b) for b in range(nz)], [])
    left += [homeward(above(i)) for i in range(1, nz)]
    for copy in left:
        copy.wait_send()

    @pl.when(z < nz - 1)
    def sent_up():
        for q in range(pieces):
            upward(q).wait_send()

    @pl.when(z > 0)
    def sent_down():
        for q in range(pieces):
            downward(q).wait_send()


def shards(
    out_gate,
    in_gate,
    conv_input,
    conv_taps,
    documents,
    out_weight,
    residual,
    norm_gain,
    expert_ids,
    route_weights,
    gate_weight,
    up_weight,
    down_weight,
):
    n_sp, nz = lax.axis_size("sp"), lax.axis_size("tp") // 2
    length, channels = conv_input.shape
    rows, width = residual.shape
    units = gate_weight.shape[2]
    capacity = max(2, (3 * rows + n_sp - 1) // n_sp)
    cap = -(-capacity // CHUNK) * CHUNK
    relayed = n_sp == 4
    pieces = nz * (rows // min(PIECE, rows))
    bf16, f32, dma = jnp.bfloat16, jnp.float32, pltpu.SemaphoreType.DMA
    hbm = pl.BlockSpec(memory_space=pltpu.HBM)
    per_z = pltpu.VMEM((nz, rows, width), bf16)
    per_z_side = per_z if relayed else pltpu.VMEM((1, CHUNK, LANES), bf16)
    slots = pltpu.VMEM((nz, n_sp, cap, width), bf16)
    return pl.pallas_call(
        functools.partial(layer_kernel, n_sp, nz, cap),
        out_shape=jax.ShapeDtypeStruct((rows, width), bf16),
        in_specs=[hbm] * 13,
        out_specs=pl.BlockSpec(memory_space=pltpu.VMEM),
        scratch_shapes=[
            pltpu.VMEM((length, channels), bf16),
            pltpu.VMEM((length, channels), bf16),
            pltpu.VMEM((length, channels), bf16),
            pltpu.VMEM(conv_taps.shape, bf16),
            pltpu.VMEM((length,), jnp.int32),
            pltpu.VMEM((rows, width), bf16),
            pltpu.VMEM((width,), bf16),
            pltpu.VMEM((2, rows), jnp.int32),
            pltpu.VMEM((2, rows), f32),
            pltpu.VMEM((width, units), bf16),
            pltpu.VMEM((width, units), bf16),
            pltpu.VMEM((units, width), bf16),
            pltpu.VMEM((HALO + length, channels), f32),
            pltpu.VMEM((HALO + length, LANES), f32),
            pltpu.VMEM((HALO, channels), f32),
            pltpu.VMEM((HALO, LANES), f32),
            pltpu.VMEM((HALO, channels), f32),
            pltpu.VMEM((HALO, LANES), f32),
            pltpu.VMEM((2 * nz, rows, channels), bf16),
            pltpu.VMEM((nz, rows, channels), bf16),
            pltpu.VMEM((2, channels, width), bf16),
            pltpu.VMEM((nz, rows, width), f32),
            per_z,
            per_z,
            per_z,
            per_z,
            per_z,
            per_z,
            pltpu.VMEM((8, rows), f32),
            pltpu.VMEM((nz, 8, rows), f32),
            pltpu.VMEM((nz, 8, rows), f32),
            per_z_side,
            slots,
            pltpu.VMEM((nz, 2, n_sp, cap, width), bf16),
            pltpu.VMEM((2 * n_sp * cap, units), bf16),
            slots,
            pltpu.VMEM((nz, 2 if relayed else n_sp, cap, width), bf16),
            per_z_side,
            per_z_side,
            pltpu.VMEM((rows, width), f32),
            per_z,
            per_z,
            dma((13,)),
            dma((2,)),
            dma((2,)),
            dma((nz,)),
            dma((nz,)),
            dma((1,)),
            dma((1,)),
            dma((1,)),
            dma((1,)),
            dma((nz,)),
            dma((nz,)),
            dma((pieces,)),
            dma((pieces,)),
            dma((pieces,)),
            dma((pieces,)),
            dma((nz,)),
            dma((nz,)),
            dma((nz, n_sp)),
            dma((nz, n_sp)),
            dma((nz,)),
            dma((nz,)),
            dma((nz,)),
            dma((nz,)),
            dma((nz, n_sp)),
            dma((nz, n_sp)),
            dma((nz,)),
            dma((nz,)),
            dma((nz,)),
            dma((nz,)),
        ],
        compiler_params=pltpu.CompilerParams(
            collective_id=0, has_side_effects=True, vmem_limit_bytes=VMEM_LIMIT
        ),
    )(
        in_gate, conv_input, out_gate, conv_taps, documents, out_weight, residual, norm_gain, expert_ids.T,
        route_weights.T, gate_weight[0], up_weight[0], down_weight[0],
    )


def solution(mesh):
    in_specs = (
        P("sp", "tp"),
        P("sp", "tp"),
        P("sp", "tp"),
        P(None, "tp"),
        P("sp"),
        P("tp", None),
        P(("sp", "tp"), None),
        P(),
        P(("sp", "tp"), None),
        P(("sp", "tp"), None),
        P("sp", None, "tp"),
        P("sp", None, "tp"),
        P("sp", "tp", None),
    )
    out_specs = P(("sp", "tp"), None)
    return jax.shard_map(shards, mesh=mesh, in_specs=in_specs, out_specs=out_specs, check_vma=False)
```

time: 129 us -> 120 us (0.930)
  Pallas kernels: 122 us -> 118 us
  other arithmetic: 2.63 us -> 0 us
  local copies, waits for them, and re-layouts: 3.79 us -> 1.67 us
    pallas_call x1, Pallas kernels: 122 us -> 118 us  [shards(): pl.pallas_call(functools.partial(layer_kernel, n_sp, nz, cap), out_shape=...]
    broadcast_in_dim x2 -> x0, local copies, waits for them, and re-layouts: 2.12 us -> none  [the longest x1 1.28 us: shards(): norm_gain[None, :]]
where the time goes in v1:
time: 120 us
  Pallas kernels  118 us (98%)
  local copies, waits for them, and re-layouts  1.67 us (1%)
    pallas_call x1, Pallas kernels, shards(): pl.pallas_call(functools.partial(layer_kernel, n_sp, nz, cap), out_shape=...  118 us

profile of v1, /device:TPU:0, one launch (start us, length us, event | category | flops | bytes accessed | tf_op | source)
XLA Modules:
  0.0 119.8 jit_solution(1705468972945591004)
XLA Ops:
  0.0 118.1 %shard_map.127 = bf16[64,2048]{1,0:T(8,128)(2,1)} custom-call(bf16[512,256]{1,0:T(8,128)(2,1)} %in_gate_hbm.1, bf16[512,256]{1,0:T(8,128)(2,1)} %conv_input_hbm.1, bf16[512,256]{1,0:T(8,128)(2,1)} %out_gate_hbm.1, bf16[3,256]{1,0:T(4,128)(2,1)} %taps_hbm.1, s32[512]{0:T(512)} %docs_hbm.1, bf16[256,2048]{1,0:T(8,128)(2,1)} %out_weight_hbm.1, ...), custom_call_target="tpu_custom_call" | custom-call | tf_op jit(solution)/shard_map/pallas_call | solution.py:611
  118.1 1.7 %copy.15 = bf16[64,2048]{1,0:T(8,128)(2,1)} copy(bf16[64,2048]{1,0:T(8,128)(2,1)} %shard_map.127) | data formatting | bytes 524288

commit v2 on v1

--- a/solution.py
+++ b/solution.py
@@ -15,10 +15,14 @@
 COLS = 512
 UNITS = 256
 HALO = 8
-PIECE = 32
-LAG = 2
+PIECE = 16
+LAG = 3
 LANES = 128
 VMEM_LIMIT = 63 * 1024 * 1024
+
+
+def turn(nz, a):
+    return (nz - 1 - a // 2) if a % 2 == 0 else a // 2
 
 
 def where_am_i():
@@ -133,6 +137,7 @@
     piece = min(PIECE, rows)
     per = rows // piece
     pieces = nz * per
+    order = [turn(nz, a) for a in range(nz)]
     greeted = greet(s, z, c, n_sp, nz)
     loads = [
         pltpu.make_async_copy(src, dst, w_sem.at[i])
@@ -209,12 +214,18 @@
     given = [
         link(gated.at[2 * b + o], other_gated.at[b], o_send.at[b], o_recv.at[b], partner) for b in range(nz)
     ]
-    lent = link(weight.at[0], weight.at[1], v_send.at[0], v_recv.at[0], partner)
-    given[nz - 1].start()
-    lent.start()
+    lent = [
+        link(
+            weight.at[0, :, pl.ds(l, COLS)], weight.at[1, :, pl.ds(l, COLS)], v_send.at[i], v_recv.at[i], partner
+        )
+        for i, l in enumerate(range(0, width, COLS))
+    ]
     for copy in halo:
         copy.start()
-    for b in range(nz - 2, 0, -1):
+    given[nz - 1].start()
+    for copy in lent:
+        copy.start()
+    for b in order[2:]:
         given[b].start()
 
     def note(i):
@@ -228,7 +239,7 @@
     side_note = link(metas, side_metas, x_send.at[0], x_recv.at[0], side_peer) if relayed else None
 
     def place(q):
-        return nz - 1 - q // per, (q % per) * piece
+        return order[q // per], (q % per) * piece
 
     def upward(q):
         b, first = place(q)
@@ -257,7 +268,12 @@
                 gated[2 * b + c], weight[0, :, cols], preferred_element_type=jnp.float32
             ) + jnp.dot(other_gated[b], weight[1, :, cols], preferred_element_type=jnp.float32)
 
-        by_columns(width, columns)
+        if b == order[0]:
+            for i, copy in enumerate(lent):
+                copy.wait_recv()
+                columns(pl.ds(i * COLS, COLS))
+        else:
+            by_columns(width, columns)
 
         @pl.when(z == b)
         def own():
@@ -266,9 +282,8 @@
 
             by_rows(0, rows, add)
 
-    lent.wait_recv()
     loads[8].wait()
-    for b in range(nz - 1, -1, -1):
+    for a, b in enumerate(order):
         if b == 0:
             for copy in halo:
                 copy.wait_recv()
@@ -277,7 +292,7 @@
             convolve(0)
             given[0].start()
         project(b)
-        for q in range((nz - 1 - b) * per, (nz - b) * per):
+        for q in range(a * per, (a + 1) * per):
 
             @pl.when(z == 0)
             def lowest(q=q):
@@ -325,8 +340,13 @@
 
         by_rows(first, piece, rows_of)
 
-    def raw_copy(b):
-        return link(nbuf.at[b], raw.at[b], g_send.at[b], g_recv.at[b], side_peer)
+    def raw_copy(b, h):
+        at = pl.ds(h * (rows // 2), rows // 2)
+        return link(nbuf.at[b, at], raw.at[b, at], g_send.at[b, h], g_recv.at[b, h], side_peer)
+
+    def send_half(b):
+        if relayed:
+            raw_copy(b, 0).start()
 
     def slot_copies(b, those=(0, 1)):
         if relayed:
@@ -341,9 +361,11 @@
             for k in range(1, n_sp)
         ]
 
+    def send_rest(b):
+        if relayed:
+            raw_copy(b, 1).start()
+
     def dispatch(b):
-        if relayed:
-            raw_copy(b).start()
         table = slot_table(metas[b], experts, cap)
 
         def columns(cols):
@@ -359,7 +381,8 @@
     def relay(b):
         if not relayed:
             return
-        raw_copy(b).wait_recv()
+        for h in range(2):
+            raw_copy(b, h).wait_recv()
         table = slot_table(side_metas[b], experts, cap)
 
         def columns(cols):
@@ -369,6 +392,18 @@
 
         by_columns(width, columns)
         slot_copies(b, (1,))[0].start()
+        forwards(b)[0].start()
+
+    def forwards(b):
+        parts = 2 if relayed else 1
+        count = n_sp // parts
+        return [
+            link(
+                gathered.at[b, 0, pl.ds(h * count, count)], gathered.at[b, 1, pl.ds(h * count, count)],
+                f_send.at[b, h], f_recv.at[b, h], partner,
+            )
+            for h in range(parts)
+        ]
 
     def unless_own(b, act_on):
         @pl.when(z != b)
@@ -396,30 +431,35 @@
             if q == 0 and relayed:
                 side_note.wait_recv()
             norm(q)
+            a = q // per
+            if q % per == max(per // 2 - 1, 0) and a >= 2:
+                unless_own(order[a - 2], relay)
+            if q % per == per // 2 - 1:
+                unless_own(order[a], send_half)
             if q % per == per - 1:
-                b = place(q)[0]
-                unless_own(b, dispatch)
-                if b < nz - 1:
-                    unless_own(b + 1, relay)
-    dispatch(z)
-    unless_own(0, relay)
-    relay(z)
+                unless_own(order[a], send_rest)
+                unless_own(order[a], dispatch)
+    own_turn = jnp.where(z >= nz // 2, 2 * (nz - 1 - z), 2 * z + 1)
 
     def at_step(j):
         if j == nz - 1:
             return z
-        return nz - 1 - j - jnp.where(j >= nz - 1 - z, 1, 0)
-
-    def forward(b):
-        return link(gathered.at[b, 0], gathered.at[b, 1], f_send.at[b], f_recv.at[b], partner)
-
-    def swap(b):
-        return link(gathered.at[b, 0], half_rx.at[b], e_send.at[b], e_recv.at[b], partner)
+        if j >= nz - 3:
+            j = jnp.where(z == nz - 1, 2 * nz - 5 - j, j)
+        a = j + jnp.where(j >= own_turn, 1, 0)
+        return jnp.where(a % 2 == 0, nz - 1 - a // 2, a // 2)
+
+    def swap(b, r):
+        cols = pl.ds(pl.multiple_of(r * COLS, COLS), COLS)
+        return link(
+            gathered.at[b, 0, :, :, cols], half_rx.at[b, :, :, cols], e_send.at[b, r], e_recv.at[b, r], partner
+        )
 
     def return_copies(b):
         if relayed:
             return [
-                link(routed.at[b, pl.ds(2, 2)], arrived.at[b], r_send.at[b, 0], r_recv.at[b, 0], cross_peer)
+                link(routed.at[b, 2 + k], arrived.at[b, k], r_send.at[b, k], r_recv.at[b, k], cross_peer)
+                for k in range(2)
             ]
         return [
             link(
@@ -435,14 +475,15 @@
         b = at_step(j)
         for copy in slot_copies(b):
             copy.wait_recv()
-        forward(b).start()
+        forwards(b)[-1].start()
 
     def expert(j):
         b = at_step(j)
         if j == 0:
             for load in loads[10:]:
                 load.wait()
-        forward(b).wait_recv()
+        for copy in forwards(b):
+            copy.wait_recv()
         half = n_sp * cap
         hidden_units = gate.shape[1]
         step = min(UNITS, hidden_units)
@@ -458,42 +499,49 @@
         lax.fori_loop(0, hidden_units // step, inner, 0)
         for copy in slot_copies(b):
             copy.wait_send()
-        forward(b).wait_send()
-
-        def outer(cols):
+        for copy in forwards(b):
+            copy.wait_send()
+
+        def outer(r, carry):
+            cols = pl.ds(pl.multiple_of(r * COLS, COLS), COLS)
             share = jnp.dot(act[...], down[:, cols], preferred_element_type=jnp.float32).astype(jnp.bfloat16)
             routed[b, :, :, cols] = share[:half].reshape(n_sp, cap, COLS)
             gathered[b, 0, :, :, cols] = share[half:].reshape(n_sp, cap, COLS)
-
-        by_columns(width, outer)
-        swap(b).start()
+            swap(b, r).start()
+            return carry
+
+        lax.fori_loop(0, width // COLS, outer, 0)
 
     def give_back(j):
         b = at_step(j)
-        swap(b).wait_recv()
-
-        def add(first, count):
-            def columns(cols):
-                at = pl.ds(first, count)
+
+        def add(first, count, waiting=False):
+            def columns(r, carry):
+                if waiting:
+                    swap(b, r).wait_recv()
+                cols, at = pl.ds(pl.multiple_of(r * COLS, COLS), COLS), pl.ds(first, count)
                 total = routed[b, at, :, cols].astype(jnp.float32) + half_rx[b, at, :, cols].astype(jnp.float32)
                 routed[b, at, :, cols] = total.astype(jnp.bfloat16)
-
-            by_columns(width, columns)
+                return carry
+
+            lax.fori_loop(0, width // COLS, columns, 0)
 
         if relayed:
-            add(2, 2)
+            add(3, 1, True)
+            return_copies(b)[1].start()
+            add(2, 1)
+            return_copies(b)[0].start()
+            add(0, 2)
         else:
-            add(0, n_sp)
-        for copy in return_copies(b):
-            copy.start()
-        if relayed:
-            add(0, 2)
+            add(0, n_sp, True)
+            for copy in return_copies(b):
+                copy.start()
 
     def relay_back(j):
         if not relayed:
             return
         b = at_step(j)
-        return_copies(b)[0].wait_recv()
+        return_copies(b)[1].wait_recv()
         weights = slot_weights(side_metas[b], experts, cap)
 
         def columns(cols):
@@ -508,11 +556,8 @@
 
     def collect(j):
         b = at_step(j)
-        if relayed:
-            side_copy(b).wait_recv()
-        else:
-            for copy in return_copies(b):
-                copy.wait_recv()
+        for copy in [return_copies(b)[0], side_copy(b)] if relayed else return_copies(b):
+            copy.wait_recv()
         weights = slot_weights(metas[b], experts, cap)
 
         def columns(cols):
@@ -533,19 +578,26 @@
         if j < nz - 1:
             homeward(b).start()
 
+    send_half(z)
+    send_rest(z)
+    unless_own(order[-2], relay)
+    dispatch(z)
     gather(0)
-    for j in range(nz):
-        if j + 1 < nz:
-            gather(j + 1)
+    expert(0)
+    unless_own(order[-1], relay)
+    for j in range(1, nz):
+        give_back(j - 1)
+        gather(j)
         expert(j)
-        if j >= 1:
-            relay_back(j - 1)
-        give_back(j)
+        if j == 1:
+            relay(z)
+        relay_back(j - 1)
+        if j == nz - 1:
+            give_back(j)
         if j >= 2:
             collect(j - 2)
     relay_back(nz - 1)
-    if nz > 1:
-        collect(nz - 2)
+    collect(nz - 2)
     collect(nz - 1)
 
     def home(i):
@@ -561,10 +613,10 @@
         out[r, :] = (hidden[z, r, :].astype(jnp.float32) + total).astype(jnp.bfloat16)
 
     by_rows(0, rows, finish)
-    left = halo + given + [lent] + [note(i) for i in range(1, nz)]
+    left = halo + given + lent + [note(i) for i in range(1, nz)]
     if relayed:
-        left += [side_note] + [raw_copy(b) for b in range(nz)] + [side_copy(b) for b in range(nz)]
-    left += [swap(b) for b in range(nz)] + sum([return_copies(b) for b in range(nz)], [])
+        left += [side_note] + [raw_copy(b, h) for b in range(nz) for h in range(2)] + [side_copy(b) for b in range(nz)]
+    left += [swap(b, r) for b in range(nz) for r in range(width // COLS)] + sum([return_copies(b) for b in range(nz)], [])
     left += [homeward(above(i)) for i in range(1, nz)]
     for copy in left:
         copy.wait_send()
@@ -663,22 +715,22 @@
             dma((nz,)),
             dma((1,)),
             dma((1,)),
-            dma((1,)),
-            dma((1,)),
+            dma((width // COLS,)),
+            dma((width // COLS,)),
             dma((nz,)),
             dma((nz,)),
             dma((pieces,)),
             dma((pieces,)),
             dma((pieces,)),
             dma((pieces,)),
-            dma((nz,)),
-            dma((nz,)),
+            dma((nz, 2)),
+            dma((nz, 2)),
             dma((nz, n_sp)),
             dma((nz, n_sp)),
-            dma((nz,)),
-            dma((nz,)),
-            dma((nz,)),
-            dma((nz,)),
+            dma((nz, 2)),
+            dma((nz, 2)),
+            dma((nz, width // COLS)),
+            dma((nz, width // COLS)),
             dma((nz, n_sp)),
             dma((nz, n_sp)),
             dma((nz,)),

time: 120 us -> 99.3 us (0.83)
  the two profiles are of different devices: /device:TPU:0 before, /device:TPU:8 now
where the time goes in v2:
time: 99.3 us; the launch traced here: 99.2 us
  Pallas kernels  97.5 us (98%)
  local copies, waits for them, and re-layouts  1.67 us (2%)
    pallas_call x1, Pallas kernels, shards(): pl.pallas_call(functools.partial(layer_kernel, n_sp, nz, cap), out_shape=...  97.5 us

profile of v2, /device:TPU:8, one launch (start us, length us, event | category | flops | bytes accessed | tf_op | source)
XLA Modules:
  0.0 99.2 jit_solution(14289260511961516003)
XLA Ops:
  0.0 97.5 %shard_map.127 = bf16[64,2048]{1,0:T(8,128)(2,1)} custom-call(bf16[512,256]{1,0:T(8,128)(2,1)} %in_gate_hbm.1, bf16[512,256]{1,0:T(8,128)(2,1)} %conv_input_hbm.1, bf16[512,256]{1,0:T(8,128)(2,1)} %out_gate_hbm.1, bf16[3,256]{1,0:T(4,128)(2,1)} %taps_hbm.1, s32[512]{0:T(512)} %docs_hbm.1, bf16[256,2048]{1,0:T(8,128)(2,1)} %out_weight_hbm.1, ...), custom_call_target="tpu_custom_call" | custom-call | tf_op jit(solution)/shard_map/pallas_call | solution.py:663
  97.5 1.7 %copy.15 = bf16[64,2048]{1,0:T(8,128)(2,1)} copy(bf16[64,2048]{1,0:T(8,128)(2,1)} %shard_map.127) | data formatting | bytes 524288
